TPU v7x, 32 devices: a whole 2x2x4 slice. The times are simulated.
32 devices in a mesh: rep: 4 (over z), fs: 4 (over y, x), tp: 2 (over core).
Axes of the slice: x: 2, y: 2, z: 4, core: 2. Of those that a mesh axis runs over, the one named last changes fastest.
Arguments:
- hidden_pre: bfloat16 [8192, 4096], P(('rep', 'fs'), 'tp'), may hold values from -6 to 6
- out_grad: bfloat16 [8192, 2048], P(('rep', 'fs')), may hold values from -8 to 8
- down_weight: bfloat16 [2048, 4096], P('fs', 'tp'), may hold values from -0.09375 to 0.09375
Outputs:
- hidden_grad: bfloat16 [8192, 4096], P(('rep', 'fs'), 'tp')
- weight_grad: float32 [2048, 4096], P('fs', 'tp')
All inputs are finite; a program needn't handle non-finite values.
Results may differ from a plain program's by a relative error of at most 0.0049.
Values may be sent and summed in bfloat16 or wider, within the bound.
A program may use at most 64 MiB of HBM per device.

v0:
```python
import math
import jax
import jax.numpy as jnp
from jax import lax
from jax.sharding import PartitionSpec as P


def body(hidden_pre, out_grad, down_weight):
    rows = hidden_pre.shape[0]
    ff_local = hidden_pre.shape[1]
    back = jnp.dot(
        out_grad,
        lax.all_gather(down_weight, "fs", axis=0, tiled=True),
        preferred_element_type=jnp.float32,
    )
    positive = jnp.maximum(hidden_pre.astype(jnp.float32), 0.0)
    hidden_grad = (2.0 * positive * back).astype(jnp.bfloat16)
    act = (positive * positive).astype(jnp.bfloat16)
    partial_value = lax.dot_general(
        out_grad, act, (((0,), (0,)), ((), ())), preferred_element_type=jnp.float32
    )
    partial_value = partial_value.astype(jnp.bfloat16)
    received = lax.all_to_all(partial_value, "fs", split_axis=0, concat_axis=0, tiled=True)
    groups = lax.axis_size("fs")
    local_sum = jnp.sum(
        received.reshape(groups, received.shape[0] // groups, ff_local), axis=0, dtype=jnp.float32
    )
    total = lax.psum(local_sum, "rep")
    tokens_all = rows * lax.axis_size("rep") * groups
    weight_grad = total * (1.0 / math.sqrt(tokens_all))
    return (hidden_grad, weight_grad)


def solution(mesh):
    placed = (P(("rep", "fs"), "tp"), P(("rep", "fs"), None), P("fs", "tp"))
    return jax.shard_map(
        body,
        mesh=mesh,
        in_specs=placed,
        out_specs=(P(("rep", "fs"), "tp"), P("fs", "tp")),
        check_vma=False,
    )
```

profile of v0, /device:TPU:0, one launch (start us, length us, event | category | flops | bytes accessed | tf_op | source)
XLA Modules:
  0.0 297.2 jit_solution(1170586137731124309)
XLA Ops:
  8.0 0.0 copy-start
  8.0 0.0 all-reduce.2.cloned.1.call-start
  8.1 1.5 copy-done
  9.6 8.3 %convolution_convert_fusion = bf16[2048,2048]{0,1:T(8,128)(2,1)} fusion(bf16[512,2048]{1,0:T(8,128)(2,1)S(1)} %copy-done, bf16[512,2048]{1,0:T(8,128)(2,1)} %param.3), kind=kOutput, calls=%fused_computation.1 | convolution fusion | flops 4303355904 | bytes 12582912 | tf_op jit(solution)/shard_map/dot_general | solution.py:19
  17.9 98.5 %all_to_all.9 = bf16[4,512,2048]{2,1,0:T(8,128)(2,1)S(1)} all-to-all(bf16[4,512,2048]{2,1,0:T(8,128)(2,1)} %bitcast.6), channel_id=1, replica_groups=mesh['rep'=4,'fs'=4,'tp'=2] {'fs'}, dimensions={0} | all-to-all | bytes 16777216 | tf_op jit(solution)/shard_map/all_to_all | solution.py:23
  116.4 3.9 %convert_reduce_fusion = f32[512,2048]{1,0:T(8,128)} fusion(bf16[4,512,2048]{2,1,0:T(8,128)(2,1)S(1)} %all_to_all.9), kind=kLoop, calls=%fused_computation | loop fusion | flops 7340032 | bytes 12582912 | tf_op jit(solution)/shard_map/reduce_sum | solution.py:25
  120.3 0.0 all-reduce.2.cloned.1.call-update
  120.3 0.0 all-gather.2.cloned.1.call-start
  120.4 0.5 all-gather.2.cloned.1.call-update
  120.9 154.4 %all-reduce.2.cloned.1.call-done = f32[512,2048]{1,0:T(8,128)} async-done(((f32[512,2048]{1,0:T(8,128)}), f32[512,2048]{1,0:T(8,128)}) %all-reduce.2.cloned.1.call-update) | async-done | bytes 4194320 | tf_op jit(solution)/shard_map/psum | solution.py:28
  275.4 5.0 %broadcast_multiply_fusion = f32[512,2048]{1,0:T(8,128)} fusion(f32[512,2048]{1,0:T(8,128)} %all-reduce.2.cloned.1.call-done), kind=kLoop, calls=%fused_computation.5 | loop fusion | flops 1048576 | bytes 8388608 | tf_op jit(solution)/shard_map/mul | solution.py:30
  280.3 0.0 all-gather.2.cloned.1.call-done
  280.3 9.5 %multiply_convert_fusion.1 = bf16[512,2048]{1,0:T(8,128)(2,1)} fusion(bf16[512,2048]{1,0:T(8,128)(2,1)} %param.3, bf16[512,2048]{1,0:T(8,128)(2,1)S(1)} %copy-done, bf16[2048,2048]{1,0:T(8,128)(2,1)} %all-gather.2.cloned.1.call-done), kind=kOutput, calls=%fused_computation.3 | convolution fusion | flops 4300210176 | bytes 14680064 | tf_op jit(solution)/shard_map/dot_general | solution.py:11
Async XLA Ops:
  8.0 1.6 copy-start
  8.0 267.3 %all-reduce.2.cloned.1.call-start = ((), (), s32[]{:S(2)}) async-start(), calls=%async_computation.2 | async-start | bytes 8388608 | tf_op jit(solution)/shard_map/psum | solution.py:28
  120.3 160.0 %all-gather.2.cloned.1.call-start = ((), (), s32[]{:S(2)}) async-start(), calls=%async_computation.1 | async-start | bytes 10485760 | tf_op jit(solution)/shard_map/all_gather | solution.py:13
Sparse Core Ops, SparseCore 0:
  120.4 154.8 all-reduce.1
Sparse Core Ops, SparseCore 1:
  122.7 87.2 all-gather.1
where the time goes:
time: 297 us
  waiting for transfers between devices  155 us (52%)
  blocking collectives  98.5 us (33%)
  matrix products  17.8 us (6%)
  between operations  15.5 us (5%)
  other arithmetic  8.83 us (3%)
    psum x1, waiting for transfers between devices, body(): total = lax.psum(local_sum, 'rep')  154 us
    all_to_all x1, blocking collectives, body(): lax.all_to_all(partial_value, 'fs', split_axis=0, concat_axis=0, tiled=True)  98.5 us
    dot_general x1, matrix products, body(): jnp.dot(out_grad, lax.all_gather(down_weight, 'fs', axis=0, tiled=True),...  9.45 us
    dot_general x1, matrix products, body(): lax.dot_general(out_grad, act, (((0,), (0,)), ((), ())), preferred_elemen...  8.35 us
  transfers between devices with their start and end apart: 2, of which 1 were waited for; matrix products, arithmetic and copies ran while one was open for 2% of the time, Pallas kernels for 0%

commit v1 on v0

--- a/solution.py
+++ b/solution.py
@@ -25,7 +25,11 @@
     local_sum = jnp.sum(
         received.reshape(groups, received.shape[0] // groups, ff_local), axis=0, dtype=jnp.float32
     )
-    total = lax.psum(local_sum, "rep")
+
+    def lines_shape(patch, mesh_ax):
+        return jnp.sum(lax.all_gather(patch, mesh_ax), axis=0)
+
+    total = lines_shape(local_sum, "rep")
     tokens_all = rows * lax.axis_size("rep") * groups
     weight_grad = total * (1.0 / math.sqrt(tokens_all))
     return (hidden_grad, weight_grad)

time: 297 us -> 494 us (1.66)
  waiting for transfers between devices: 155 us -> 283 us
  blocking collectives: 98.5 us -> 159 us
  other arithmetic: 8.83 us -> 19 us
    all_gather x0 -> x1, waiting for transfers between devices: none -> 279 us  [lines_shape(): return jnp.sum(lax.all_gather(patch, mesh_ax), axis=0)]
    psum x1 -> x0, waiting for transfers between devices: 154 us -> none  [body(): total = lax.psum(local_sum, 'rep')]
    all_to_all x1, blocking collectives: 98.5 us -> 159 us  [body(): lax.all_to_all(partial_value, 'fs', split_axis=0, concat_axis=0, tiled=True)]
    reduce_sum x0 -> x1, other arithmetic: none -> 10.2 us  [lines_shape(): return jnp.sum(lax.all_gather(patch, mesh_ax), axis=0)]
  transfers between devices with their start and end apart: 2 -> 2, of which waited for: 1 -> 2; matrix products, arithmetic and copies ran while one was open for 2% -> 4% of each run, Pallas kernels for 0% -> 0%
where the time goes in v1:
time: 494 us; the launch traced here: 493 us
  waiting for transfers between devices  283 us (57%)
  blocking collectives  159 us (32%)
  other arithmetic  19 us (4%)
  matrix products  17.8 us (4%)
  between operations  14 us (3%)
    all_gather x1, waiting for transfers between devices, lines_shape(): return jnp.sum(lax.all_gather(patch, mesh_ax), axis=0)  279 us
    all_to_all x1, blocking collectives, body(): lax.all_to_all(partial_value, 'fs', split_axis=0, concat_axis=0, tiled=True)  159 us
    reduce_sum x1, other arithmetic, lines_shape(): return jnp.sum(lax.all_gather(patch, mesh_ax), axis=0)  10.2 us
  transfers between devices with their start and end apart: 2, of which 2 were waited for; matrix products, arithmetic and copies ran while one was open for 4% of the time, Pallas kernels for 0%

profile of v1, /device:TPU:0, one launch (start us, length us, event | category | flops | bytes accessed | tf_op | source)
XLA Modules:
  0.0 493.3 jit_solution(6879388479122855075)
XLA Ops:
  7.2 0.0 copy-start
  7.2 0.0 all-gather.4.cloned.1.call-start
  7.2 0.7 all-gather.4.cloned.1.call-update
  7.9 0.0 all-gather.6.cloned.1.call-start
  8.0 0.8 copy-done
  8.8 8.3 %convolution_convert_fusion = bf16[2048,2048]{0,1:T(8,128)(2,1)} fusion(bf16[512,2048]{1,0:T(8,128)(2,1)S(1)} %copy-done, bf16[512,2048]{1,0:T(8,128)(2,1)} %param.3), kind=kOutput, calls=%fused_computation.1 | convolution fusion | flops 4303355904 | bytes 12582912 | tf_op jit(solution)/shard_map/dot_general | solution.py:19
  17.1 158.8 %all_to_all.9 = bf16[4,512,2048]{2,1,0:T(8,128)(2,1)S(1)} all-to-all(bf16[4,512,2048]{2,1,0:T(8,128)(2,1)} %bitcast.8), channel_id=1, replica_groups=mesh['rep'=4,'fs'=4,'tp'=2] {'fs'}, dimensions={0} | all-to-all | bytes 16777216 | tf_op jit(solution)/shard_map/all_to_all | solution.py:23
  175.9 3.9 convert_reduce_fusion
  179.7 0.0 all-gather.6.cloned.1.call-update
  179.8 2.6 all-gather.4.cloned.1.call-done
  182.4 9.5 %multiply_convert_fusion.1 = bf16[512,2048]{1,0:T(8,128)(2,1)} fusion(bf16[512,2048]{1,0:T(8,128)(2,1)} %param.3, bf16[512,2048]{1,0:T(8,128)(2,1)S(1)} %copy-done, bf16[2048,2048]{1,0:T(8,128)(2,1)} %all-gather.4.cloned.1.call-done), kind=kOutput, calls=%fused_computation.3 | convolution fusion | flops 4300210176 | bytes 14680064 | tf_op jit(solution)/shard_map/dot_general | solution.py:11
  191.8 279.5 %all-gather.6.cloned.1.call-done = f32[2048,2048]{1,0:T(8,128)} async-done(((f32[512,2048]{1,0:T(8,128)}), f32[2048,2048]{1,0:T(8,128)}) %all-gather.6.cloned.1.call-update) | async-done | bytes 16777232 | tf_op jit(solution)/shard_map/all_gather | solution.py:30
  471.3 10.2 %reduce_sum.19 = f32[512,2048]{1,0:T(8,128)} reduce(f32[4,512,2048]{2,1,0:T(8,128)} %bitcast.7, f32[]{:T(128)} %constant.3.clone.1), dimensions={0}, to_apply=%region_1.0 | reduce | flops 3145728 | bytes 20971524 | tf_op jit(solution)/shard_map/reduce_sum | solution.py:30
  481.5 5.0 %broadcast_multiply_fusion = f32[512,2048]{1,0:T(8,128)} fusion(f32[512,2048]{1,0:T(8,128)} %reduce_sum.19), kind=kLoop, calls=%fused_computation.5 | loop fusion | flops 1048576 | bytes 8388608 | tf_op jit(solution)/shard_map/mul | solution.py:34
Async XLA Ops:
  7.2 1.6 copy-start
  7.2 175.2 %all-gather.4.cloned.1.call-start = ((), (), s32[]{:S(2)}) async-start(), calls=%async_computation.1 | async-start | bytes 10485760 | tf_op jit(solution)/shard_map/all_gather | solution.py:13
  7.9 463.4 %all-gather.6.cloned.1.call-start = ((), (), s32[]{:S(2)}) async-start(), calls=%async_computation.2 | async-start | bytes 20971520 | tf_op jit(solution)/shard_map/all_gather | solution.py:30
Sparse Core Ops, SparseCore 0:
  9.8 172.5 all-gather.3
  184.5 286.7 all-gather.5
